TPU v7x, 32 devices: a whole 2x2x4 slice. The times are simulated.
32 devices in a mesh: fs: 4 (over y, x), tp: 8 (over z, core).
Axes of the slice: x: 2, y: 2, z: 4, core: 2. Of those that a mesh axis runs over, the one named last changes fastest.
Arguments:
- hidden_in: bfloat16 [6144, 4096], P('fs', 'tp'), may hold values from -6 to 6
- forget_pre: bfloat16 [6144, 2048], P('fs', 'tp'), may hold values from -8 to 8
- forget_cot: bfloat16 [6144, 2048], P('fs', 'tp'), may hold values from -0.4375 to 0.4375
- lower_bound: float32 [2048], P('tp'), may hold values from 0.05 to 0.9
- head_out: bfloat16 [6144, 2048], P('fs', 'tp'), may hold values from -6 to 6
- out_cot: bfloat16 [6144, 4096], P('fs', 'tp'), may hold values from -0.109375 to 0.109375
- basis_forget: bfloat16 [2048, 256], replicated, may hold values from -0.37565048 to 0.37565048
- basis_output: bfloat16 [2048, 256], replicated, may hold values from -0.37565048 to 0.37565048
- weight_forget: float32 [2048, 4096], P('fs', 'tp'), may hold values from -0.09375 to 0.09375
- weight_output: float32 [4096, 2048], P('tp', 'fs'), may hold values from -0.125 to 0.125
- mean_forget: float32 [256, 4096], P('fs', 'tp'), may hold values from -3.5 to 3.5
- var_forget: float32 [256, 4096], P('fs', 'tp'), may hold values from 0.003 to 0.05
- mean_output: float32 [256, 4096], P('fs', 'tp'), may hold values from -3.5 to 3.5
- var_output: float32 [256, 4096], P('fs', 'tp'), may hold values from 0.003 to 0.05
Outputs:
- step_forget: float32 [2048, 4096], P('fs', 'tp')
- step_output: float32 [4096, 2048], P('tp', 'fs')
- new_forget: float32 [2048, 4096], P('fs', 'tp')
- new_output: float32 [4096, 2048], P('tp', 'fs')
- mean_forget_new: float32 [256, 4096], P('fs', 'tp')
- var_forget_new: float32 [256, 4096], P('fs', 'tp')
- mean_output_new: float32 [256, 4096], P('fs', 'tp')
- var_output_new: float32 [256, 4096], P('fs', 'tp')
- copy_forget: bfloat16 [2048, 4096], P(None, 'tp')
- copy_output: bfloat16 [4096, 2048], P('tp')
All inputs are finite; a program needn't handle non-finite values.
Results may differ from a plain program's by a relative error of at most 0.014.
Values may be sent and summed in bfloat16 or wider, within the bound.
A program may use at most 64 MiB of HBM per device.

v0:
```python
import jax
import jax.numpy as jnp
from jax import lax
from jax.sharding import PartitionSpec as P

D = 4096
HW = 2048


beta_one = 0.9
beta_two = 0.99
adam_eps = 1e-08
norm_eps = 1e-06
step_rate = 0.02


def moment_update(mean, var, proj):
    mean_new = beta_one * mean + (1.0 - beta_one) * proj
    var_new = beta_two * var + (1.0 - beta_two) * proj * proj
    return (mean_new, var_new, mean_new / (jnp.sqrt(var_new) + adam_eps))


def split_product(coords, tokens_data):
    upper = coords.astype(jnp.bfloat16)
    lower = (coords - upper.astype(jnp.float32)).astype(jnp.bfloat16)
    first = jnp.einsum("tr,td->rd", upper, tokens_data, preferred_element_type=jnp.float32)
    second = jnp.einsum("tr,td->rd", lower, tokens_data, preferred_element_type=jnp.float32)
    return first + second


def per_device(
    hidden_in,
    forget_pre,
    forget_cot,
    lower_bound,
    head_out,
    out_cot,
    basis_forget,
    basis_output,
    weight_forget,
    weight_output,
    mean_forget,
    var_forget,
    mean_output,
    var_output,
):
    highest = lax.Precision.HIGHEST
    fs_rank = lax.axis_index("fs")
    tp_rank = lax.axis_index("tp")
    unit_count = forget_pre.shape[1]
    feat_cols = hidden_in.shape[1]
    head_rows = weight_forget.shape[0]
    sigmoid_z = jax.nn.sigmoid(forget_pre.astype(jnp.float32))
    keep_rate = 1.0 - lower_bound
    forget_val = lower_bound + keep_rate * sigmoid_z
    gate_grad = (
        forget_cot.astype(jnp.float32) * keep_rate * sigmoid_z * (1.0 - sigmoid_z) / forget_val
    ).astype(jnp.bfloat16)
    rows_forget = lax.dynamic_slice_in_dim(basis_forget, fs_rank * head_rows, head_rows, 0).astype(
        jnp.float32
    )
    rows_output = lax.dynamic_slice_in_dim(basis_output, fs_rank * head_rows, head_rows, 0).astype(
        jnp.float32
    )
    local_forget = lax.dynamic_slice_in_dim(basis_forget, tp_rank * unit_count, unit_count, 0)
    local_output = lax.dynamic_slice_in_dim(basis_output, tp_rank * unit_count, unit_count, 0)
    coords_forget = jnp.dot(gate_grad, local_forget, preferred_element_type=jnp.float32)
    coords_output = jnp.dot(head_out, local_output, preferred_element_type=jnp.float32)
    coords_forget, coords_output = lax.psum((coords_forget, coords_output), "tp")
    part_forget = split_product(coords_forget, hidden_in)
    part_output = split_product(coords_output, out_cot)
    proj = lax.psum_scatter(
        jnp.concatenate([part_forget, part_output], axis=1), "fs", scatter_dimension=0, tiled=True
    )
    mean_f, var_f, dir_forget = moment_update(mean_forget, var_forget, proj[:, :feat_cols])
    mean_o, var_o, dir_output = moment_update(mean_output, var_output, proj[:, feat_cols:])
    dir_forget, dir_output = (
        lax.all_gather(dir_forget, "fs", axis=0, tiled=True),
        lax.all_gather(dir_output, "fs", axis=0, tiled=True),
    )
    upd_forget = jnp.dot(rows_forget, dir_forget, precision=highest)
    upd_output = jnp.dot(rows_output, dir_output, precision=highest)
    total = float(HW * D)
    sum_forget, sum_output = lax.psum(
        (jnp.sum(upd_forget * upd_forget), jnp.sum(upd_output * upd_output)), ("fs", "tp")
    )
    step_forget = upd_forget * lax.rsqrt(sum_forget / total + norm_eps)
    step_output = (upd_output * lax.rsqrt(sum_output / total + norm_eps)).T
    new_forget = weight_forget - step_rate * step_forget
    new_output = weight_output - step_rate * step_output
    copy_forget, copy_output = (
        lax.all_gather(new_forget.astype(jnp.bfloat16), "fs", axis=0, tiled=True),
        lax.all_gather(new_output.astype(jnp.bfloat16), "fs", axis=1, tiled=True),
    )
    return (
        step_forget,
        step_output,
        new_forget,
        new_output,
        mean_f,
        var_f,
        mean_o,
        var_o,
        copy_forget,
        copy_output,
    )


def solution(mesh):
    return jax.shard_map(
        per_device,
        mesh=mesh,
        in_specs=(
            P("fs", "tp"),
            P("fs", "tp"),
            P("fs", "tp"),
            P("tp"),
            P("fs", "tp"),
            P("fs", "tp"),
            P(),
            P(),
            P("fs", "tp"),
            P("tp", "fs"),
            P("fs", "tp"),
            P("fs", "tp"),
            P("fs", "tp"),
            P("fs", "tp"),
        ),
        out_specs=(
            P("fs", "tp"),
            P("tp", "fs"),
            P("fs", "tp"),
            P("tp", "fs"),
            P("fs", "tp"),
            P("fs", "tp"),
            P("fs", "tp"),
            P("fs", "tp"),
            P(None, "tp"),
            P("tp", None),
        ),
        check_vma=False,
    )
```

profile of v0, /device:TPU:0, one launch (start us, length us, event | category | flops | bytes accessed | tf_op | source)
XLA Modules:
  0.0 282.4 jit_solution(18277025858053126377)
XLA Ops:
  7.3 0.8 broadcast_subtract_fusion
  8.1 2.8 convolution_bitcast_fusion
  10.9 3.0 %fusion = f32[1536,256]{1,0:T(8,128)} fusion(bf16[1536,256]{1,0:T(8,128)(2,1)S(1)} %copy-done.10, bf16[1536,256]{1,0:T(8,128)(2,1)S(1)} %copy-done.11, f32[256]{0:T(256)S(1)} %copy-done.9, f32[256]{0:T(256)S(1)} %broadcast_subtract_fusion, bf16[2048,256]{1,0:T(8,128)(2,1)} %param.20, s32[]{:T(128)S(6)} %select_n.9), kind=kOutput, calls=%fused_computation.12 | convolution fusion | flops 206438400 | bytes 3278852 | tf_op jit(solution)/shard_map/dot_general | solution.py:67
  13.9 79.7 %all-reduce.4.cloned.1.call-done = (f32[1536,256]{0,1:T(8,128)}, f32[1536,256]{1,0:T(8,128)}) async-done(((f32[1536,256]{0,1:T(8,128)}, f32[1536,256]{1,0:T(8,128)}), (f32[1536,256]{0,1:T(8,128)}, f32[1536,256]{1,0:T(8,128)})) %all-reduce.4.cloned.1.call-update) | async-done | bytes 3145744 | tf_op jit(solution)/shard_map/psum | solution.py:69
  93.7 2.1 fusion.2
  95.8 0.6 convolution_add_fusion
  96.4 0.8 copy-done.1
  97.7 0.6 fusion.5
  98.3 0.6 convolution_add_fusion.1
  98.9 1.1 pad_maximum_fusion
  100.1 28.0 %reduce-scatter.2.cloned.1.call-done = f32[64,1024]{1,0:T(8,128)} async-done(((f32[256,1024]{1,0:T(8,128)}), f32[64,1024]{1,0:T(8,128)}) %reduce-scatter.2.cloned.1.call-update) | async-done | bytes 262160 | tf_op jit(solution)/shard_map/reduce_scatter | solution.py:72
  128.0 1.9 add_divide_fusion
  129.9 10.1 %all_gather.13 = f32[256,512]{1,0:T(8,128)S(1)} all-gather(f32[64,512]{1,0:T(8,128)S(1)} %get-tuple-element.20), channel_id=1, replica_groups=mesh['fs'=4,'tp'=8] {'fs'}, dimensions={0}, use_global_device_ids=true | all-gather | bytes 655360 | tf_op jit(solution)/shard_map/all_gather | solution.py:79
  140.0 9.7 %all_gather.12 = f32[256,512]{1,0:T(8,128)S(1)} all-gather(f32[64,512]{1,0:T(8,128)S(1)} %get-tuple-element.26), channel_id=1, replica_groups=mesh['fs'=4,'tp'=8] {'fs'}, dimensions={0}, use_global_device_ids=true | all-gather | bytes 655360 | tf_op jit(solution)/shard_map/all_gather | solution.py:78
  149.7 2.3 multiply_reduce_fusion.1
  152.0 3.2 %multiply_reduce_fusion = (f32[]{:T(128)}, f32[512,512]{1,0:T(8,128)}) fusion(f32[256,512]{1,0:T(8,128)S(1)} %all_gather.13, bf16[2048,256]{1,0:T(8,128)(2,1)} %param.21, s32[]{:T(128)S(6)} %select_n.8), kind=kOutput, calls=%fused_computation.10 | convolution fusion | flops 805830656 | bytes 1835016 | tf_op jit(solution)/shard_map/dot_general | solution.py:82
  155.1 39.5 %all-reduce = (f32[]{:T(128)}, f32[]{:T(128)}) all-reduce(f32[]{:T(128)} %get-tuple-element.29, f32[]{:T(128)} %get-tuple-element.31), channel_id=1, replica_groups=mesh['fs'=4,'tp'=8] {'fs','tp'}, use_global_device_ids=true, to_apply=%region_4.0 | all-reduce | flops 2 | bytes 16 | tf_op jit(solution)/shard_map/psum | solution.py:84
  195.4 3.1 %fusion.21 = (bf16[512,512]{1,0:T(8,128)(2,1)}, f32[512,512]{1,0:T(8,128)}, f32[512,512]{1,0:T(8,128)}) fusion(f32[512,512]{1,0:T(8,128)} %param.22, f32[512,512]{1,0:T(8,128)S(1)} %get-tuple-element.30, f32[]{:T(128)S(6)} %rsqrt.6), kind=kLoop, calls=%fused_computation.41 | loop fusion | flops 1048576 | bytes 4718596 | tf_op jit(solution)/shard_map/convert_element_type | solution.py:92
  198.5 1.6 copy.24
  200.8 3.1 %fusion.20 = (bf16[512,512]{1,0:T(8,128)(2,1)}, f32[512,512]{1,0:T(8,128)}, f32[512,512]{1,0:T(8,128)}) fusion(f32[512,512]{1,0:T(8,128)} %param.23, f32[512,512]{0,1:T(8,128)S(1)} %copy.24, f32[]{:T(128)S(6)} %rsqrt.7), kind=kLoop, calls=%fused_computation.40 | loop fusion | flops 1048576 | bytes 4718596 | tf_op jit(solution)/shard_map/convert_element_type | solution.py:93
  203.9 30.1 %all-gather.3.cloned.1.call-done = bf16[2048,512]{1,0:T(8,128)(2,1)} async-done(((bf16[512,512]{1,0:T(8,128)(2,1)}), bf16[2048,512]{1,0:T(8,128)(2,1)}) %all-gather.3.cloned.1.call-update) | async-done | bytes 2097168 | tf_op jit(solution)/shard_map/all_gather | solution.py:92
  234.0 37.3 %all-gather.5.cloned.1.call-done = bf16[512,2048]{1,0:T(8,128)(2,1)} async-done(((bf16[512,512]{1,0:T(8,128)(2,1)}), bf16[512,2048]{1,0:T(8,128)(2,1)}) %all-gather.5.cloned.1.call-update) | async-done | bytes 2097168 | tf_op jit(solution)/shard_map/all_gather | solution.py:93
  271.4 3.2 %copy.29 = bf16[2048,512]{1,0:T(8,128)(2,1)} copy(bf16[2048,512]{1,0:T(8,128)(2,1)} %all-gather.3.cloned.1.call-done) | data formatting | bytes 4194304
  274.6 1.3 copy.30
  (31 shorter events, 0.8 us)
Async XLA Ops:
  7.2 86.5 %copy-start = (bf16[1536,512]{1,0:T(8,128)(2,1)S(1)}, bf16[1536,512]{1,0:T(8,128)(2,1)}, u32[]{:S(2)}) copy-start(bf16[1536,512]{1,0:T(8,128)(2,1)} %param.19) | copy-start | bytes 4718596
  7.2 3.7 %copy-start.9 = (f32[256]{0:T(256)S(1)}, f32[256]{0:T(256)}, u32[]{:S(2)}) copy-start(f32[256]{0:T(256)} %param.17) | copy-start | bytes 3076
  7.2 3.7 %copy-start.11 = (bf16[1536,256]{1,0:T(8,128)(2,1)S(1)}, bf16[1536,256]{1,0:T(8,128)(2,1)}, u32[]{:S(2)}) copy-start(bf16[1536,256]{1,0:T(8,128)(2,1)} %param.16) | copy-start | bytes 2359300
  7.2 3.7 %copy-start.10 = (bf16[1536,256]{1,0:T(8,128)(2,1)S(1)}, bf16[1536,256]{1,0:T(8,128)(2,1)}, u32[]{:S(2)}) copy-start(bf16[1536,256]{1,0:T(8,128)(2,1)} %param.15) | copy-start | bytes 2359300
  7.2 86.4 %all-reduce.4.cloned.1.call-start = ((), (), s32[]{:S(2)}) async-start(), calls=%async_computation.4 | async-start | bytes 6291456 | tf_op jit(solution)/shard_map/psum | solution.py:69
  13.9 114.1 %reduce-scatter.2.cloned.1.call-start = ((), (), s32[]{:S(2)}) async-start(), calls=%async_computation.1 | async-start | bytes 1310720 | tf_op jit(solution)/shard_map/reduce_scatter | solution.py:72
  93.7 2.1 copy-start.3
  95.8 1.4 copy-start.1
  95.8 1.9 copy-start.2
  98.9 29.2 %copy-start.5 = (f32[64,512]{1,0:T(8,128)S(1)}, f32[64,512]{1,0:T(8,128)}, u32[]{:S(2)}) copy-start(f32[64,512]{1,0:T(8,128)} %param.27) | copy-start | bytes 393220
  98.9 29.2 %copy-start.6 = (f32[64,512]{1,0:T(8,128)S(1)}, f32[64,512]{1,0:T(8,128)}, u32[]{:S(2)}) copy-start(f32[64,512]{1,0:T(8,128)} %param.26) | copy-start | bytes 393220
  98.9 29.1 %copy-start.7 = (f32[64,512]{1,0:T(8,128)S(1)}, f32[64,512]{1,0:T(8,128)}, u32[]{:S(2)}) copy-start(f32[64,512]{1,0:T(8,128)} %param.25) | copy-start | bytes 393220
  98.9 29.1 %copy-start.8 = (f32[64,512]{1,0:T(8,128)S(1)}, f32[64,512]{1,0:T(8,128)}, u32[]{:S(2)}) copy-start(f32[64,512]{1,0:T(8,128)} %param.24) | copy-start | bytes 393220
  100.0 134.0 %all-gather.3.cloned.1.call-start = ((), (), s32[]{:S(2)}) async-start(), calls=%async_computation.2 | async-start | bytes 2621440 | tf_op jit(solution)/shard_map/all_gather | solution.py:92
  198.5 72.9 %all-gather.5.cloned.1.call-start = ((), (), s32[]{:S(2)}) async-start(), calls=%async_computation.3 | async-start | bytes 2621440 | tf_op jit(solution)/shard_map/all_gather | solution.py:93
  271.4 3.2 %copy-start.4 = (bf16[512,2048]{1,0:T(8,128)(2,1)S(1)}, bf16[512,2048]{1,0:T(8,128)(2,1)}, u32[]{:S(2)}) copy-start(bf16[512,2048]{1,0:T(8,128)(2,1)} %all-gather.5.cloned.1.call-done) | copy-start | bytes 6291460
Sparse Core Ops, SparseCore 0:
  14.0 79.5 all-reduce.3
  100.1 27.8 reduce-scatter.1
  198.6 35.3 all-gather.2
  236.3 35.0 all-gather.4
where the time goes:
time: 283 us; the launch traced here: 282 us
  waiting for transfers between devices  175 us (62%)
  blocking collectives  59.3 us (21%)
  between operations  15.3 us (5%)
  matrix products  15.1 us (5%)
  other arithmetic  9.91 us (4%)
  local copies, waits for them, and re-layouts  7.41 us (3%)
    psum x1, waiting for transfers between devices, per_device(): lax.psum((coords_forget, coords_output), 'tp')  79.7 us
    psum x1, blocking collectives, per_device(): lax.psum((jnp.sum(upd_forget * upd_forget), jnp.sum(upd_output * upd_outp...  39.5 us
    all_gather x1, waiting for transfers between devices, per_device(): lax.all_gather(new_output.astype(jnp.bfloat16), 'fs', axis=1, tiled=True)  37.3 us
    all_gather x1, waiting for transfers between devices, per_device(): lax.all_gather(new_forget.astype(jnp.bfloat16), 'fs', axis=0, tiled=True)  30.1 us
    reduce_scatter x1, waiting for transfers between devices, per_device(): lax.psum_scatter(jnp.concatenate([part_forget, part_output], axis=1), 'fs...  28 us
    all_gather x1, blocking collectives, per_device(): lax.all_gather(dir_output, 'fs', axis=0, tiled=True)  10.1 us
    all_gather x1, blocking collectives, per_device(): lax.all_gather(dir_forget, 'fs', axis=0, tiled=True)  9.67 us
    unnamed x26, local copies, waits for them, and re-layouts  5.86 us
  transfers between devices with their start and end apart: 4, of which 4 were waited for; matrix products, arithmetic and copies ran while one was open for 2% of the time, Pallas kernels for 0%

commit v1 on v0

--- a/solution.py
+++ b/solution.py
@@ -1,11 +1,16 @@
+import functools
+
 import jax
 import jax.numpy as jnp
 from jax import lax
+from jax.experimental import pallas as pl
+from jax.experimental.pallas import tpu as pltpu
 from jax.sharding import PartitionSpec as P
 
-D = 4096
-HW = 2048
-
+MESH = pl.DeviceIdType.MESH
+LANES = 128
+SUBLANES = 8
+CORES = 2
 
 beta_one = 0.9
 beta_two = 0.99
@@ -18,6 +23,422 @@
     mean_new = beta_one * mean + (1.0 - beta_one) * proj
     var_new = beta_two * var + (1.0 - beta_two) * proj * proj
     return (mean_new, var_new, mean_new / (jnp.sqrt(var_new) + adam_eps))
+
+
+def comm_kernel(
+    n_fs,
+    n_tp,
+    total,
+    ho_h, fp_h, fc_h, lb_ref, bo_h, bf_h, wo_h, wf_h, oc_h, hi_h, mo_h, vo_h, mf_h, vf_h,
+    dir_ref, proj_ref, scale_ref, wall_o, wall_f,
+    ho, fp, fc, bo, bf, wo, wf, oc, hi, mo, vo, mf, vf,
+    own, psnd, prcv, zsnd, zrcv, coords, gsnd, grcv, pown, wsnd, ssnd, srcv, gram,
+    ld, pair_s, pair_r, z_s, z_r, ag_s, ag_r, pp_s, pp_r, g_s, g_r, d_s, d_r, w_s, w_r, wl, s_s, s_r,
+):
+    n_z = n_tp // CORES
+    fs = lax.axis_index("fs")
+    tp = lax.axis_index("tp")
+    z = tp // CORES
+    core = lax.rem(tp, CORES)
+    partner = z * CORES + (1 - core)
+    tokens, units = ho.shape
+    rank = bo.shape[1]
+    half = tokens // CORES
+    quarter = half // n_z
+    part = rank // n_fs
+
+    def z_peer(d):
+        return lax.rem(z + d, n_z) * CORES + core
+
+    def fs_peer(d):
+        return lax.rem(fs + d, n_fs)
+
+    def remote(src, dst, ssem, rsem, **where):
+        return pltpu.make_async_remote_copy(
+            src_ref=src, dst_ref=dst, send_sem=ssem, recv_sem=rsem,
+            device_id=where, device_id_type=MESH,
+        )
+
+    loads = [
+        pltpu.make_async_copy(s, d, ld.at[i])
+        for i, (s, d) in enumerate((
+            (ho_h, ho), (bo_h, bo), (wo_h, wo), (wf_h, wf), (fp_h, fp), (fc_h, fc), (bf_h, bf),
+            (oc_h, oc), (hi_h, hi), (mo_h, mo), (vo_h, vo), (mf_h, mf), (vf_h, vf),
+        ))
+    ]
+    (l_ho, l_bo, l_wo, l_wf, l_fp, l_fc, l_bf, l_oc, l_hi, l_mo, l_vo, l_mf, l_vf) = loads
+    for l in loads:
+        l.start()
+
+    barrier = pltpu.get_barrier_semaphore()
+    for d in range(1, n_tp):
+        pl.semaphore_signal(barrier, inc=1, device_id={"tp": lax.rem(tp + d, n_tp)}, device_id_type=MESH)
+    for d in range(1, n_fs):
+        pl.semaphore_signal(barrier, inc=1, device_id={"fs": fs_peer(d)}, device_id_type=MESH)
+
+    l_wo.wait()
+    wsnd[0] = wo[...].astype(jnp.bfloat16)
+    l_wf.wait()
+    wsnd[1] = wf[...].astype(jnp.bfloat16)
+
+    def rows_at(which, i):
+        return pl.ds(pl.multiple_of(which * half + i * quarter, quarter), quarter)
+
+    def local_rows(b):
+        return b[pl.ds(pl.multiple_of(tp * units, units), units), :]
+
+    l_ho.wait()
+    l_bo.wait()
+
+    def coord_o(which, i):
+        return jnp.dot(ho[rows_at(which, i), :], local_rows(bo), preferred_element_type=jnp.float32)
+
+    l_fp.wait()
+    l_fc.wait()
+    l_bf.wait()
+
+    def coord_f(which, i):
+        rows = rows_at(which, i)
+        e = jnp.exp(-fp[rows, :].astype(jnp.float32))
+        lb = lb_ref[...]
+        gate = fc[rows, :].astype(jnp.float32) * (1.0 - lb) * e / ((1.0 + e) * (1.0 + lb * e))
+        return jnp.dot(gate.astype(jnp.bfloat16), local_rows(bf), preferred_element_type=jnp.float32)
+
+    coord = (coord_o, coord_f)
+    pair = [remote(psnd.at[m], prcv.at[m], pair_s.at[m], pair_r.at[m], tp=partner) for m in range(2)]
+
+    def away(m):
+        def body(i, carry):
+            psnd[m, pl.ds(pl.multiple_of(i * quarter, quarter), quarter), :] = coord[m](1 - core, i).astype(
+                jnp.bfloat16
+            )
+            return carry
+
+        lax.fori_loop(0, n_z, body, 0)
+
+    def home(m):
+        def body(i, carry):
+            own[m, pl.ds(pl.multiple_of(i * quarter, quarter), quarter), :] = coord[m](core, i)
+            return carry
+
+        lax.fori_loop(0, n_z, body, 0)
+
+    away(0)
+    pl.semaphore_wait(barrier, n_tp - 1 + n_fs - 1)
+    weights = []
+    for m, wall in ((0, wall_o), (1, wall_f)):
+        for d in range(1, n_fs):
+            c = remote(wsnd.at[m], wall.at[fs], w_s.at[m, d], w_r.at[m, d], fs=fs_peer(d))
+            weights.append(c)
+            c.start()
+        c = pltpu.make_async_copy(wsnd.at[m], wall.at[fs], wl.at[m])
+        c.start()
+        weights.append(c)
+    pair[0].start()
+    away(1)
+    pair[1].start()
+    home(0)
+
+    def chunk(ref, m, j):
+        return ref.at[m, pl.ds(pl.multiple_of(j * quarter, quarter), quarter)]
+
+    order = sorted(range(1, n_z), key=lambda d: abs(d - n_z // 2))
+
+    def scatter(m):
+        pair[m].wait_recv()
+
+        def body(i, carry):
+            rows = pl.ds(pl.multiple_of(i * quarter, quarter), quarter)
+            added = own[m, rows, :] + prcv[m, rows, :].astype(jnp.float32)
+            own[m, rows, :] = added
+            zsnd[m, rows, :] = added.astype(jnp.bfloat16)
+            return carry
+
+        lax.fori_loop(0, n_z, body, 0)
+        sends = []
+        for d in order:
+            c = remote(
+                chunk(zsnd, m, lax.rem(z + d, n_z)), zrcv.at[m, d], z_s.at[m, d], z_r.at[m, d], tp=z_peer(d)
+            )
+            c.start()
+            sends.append(c)
+        return sends
+
+    scat = [scatter(0)]
+    home(1)
+    scat.append(scatter(1))
+
+    for m, b in ((0, bo), (1, bf)):
+        g = lax.dot_general(b[...], b[...], (((0,), (0,)), ((), ())), preferred_element_type=jnp.float32)
+        upper = g.astype(jnp.bfloat16)
+        gram[m, 0] = upper
+        gram[m, 1] = (g - upper.astype(jnp.float32)).astype(jnp.bfloat16)
+
+    def spot(which, j):
+        return pl.ds(pl.multiple_of(which * half + j * quarter, quarter), quarter)
+
+    def forward(m, d):
+        rows = coords.at[m, spot(core, lax.rem(z + n_z - d, n_z))]
+        return remote(rows, rows, pp_s.at[m, d], pp_r.at[m, d], tp=partner)
+
+    def gather(m):
+        for c in scat[m]:
+            c.wait_recv()
+        sums = own[m, pl.ds(pl.multiple_of(z * quarter, quarter), quarter), :]
+        for d in range(1, n_z):
+            sums = sums + zrcv[m, d].astype(jnp.float32)
+        coords[m, spot(core, z), :] = sums.astype(jnp.bfloat16)
+        rows = coords.at[m, spot(core, z)]
+        sends = []
+        for d in order:
+            c = remote(rows, rows, ag_s.at[m, d], ag_r.at[m, d], tp=z_peer(d))
+            c.start()
+            sends.append((d, c))
+        f = forward(m, 0)
+        f.start()
+        return sends, [f]
+
+    gat = [gather(0), gather(1)]
+
+    data = ((oc, l_oc), (hi, l_hi))
+
+    def project(m):
+        sends, fwd = gat[m]
+        for d, c in sends:
+            c.wait_recv()
+            f = forward(m, d)
+            f.start()
+            fwd.append(f)
+        data[m][1].wait()
+        for f in fwd:
+            f.wait_recv()
+        proj = lax.dot_general(
+            coords[m], data[m][0][...], (((0,), (0,)), ((), ())), preferred_element_type=jnp.float32
+        )
+        pown[m] = proj
+        gsnd[m] = proj.astype(jnp.bfloat16)
+        out = []
+        for d in range(1, n_fs):
+            c = remote(
+                gsnd.at[m, pl.ds(pl.multiple_of(fs_peer(d) * part, part), part)],
+                grcv.at[m, d], g_s.at[m, d], g_r.at[m, d], fs=fs_peer(d),
+            )
+            c.start()
+            out.append(c)
+        return out
+
+    red = [project(0), project(1)]
+    moments = (((mo, l_mo), (vo, l_vo)), ((mf, l_mf), (vf, l_vf)))
+    own_ranks = pl.ds(pl.multiple_of(fs * part, part), part)
+
+    def direct(m):
+        for c in red[m]:
+            c.wait_recv()
+        proj = pown[m, own_ranks, :]
+        for d in range(1, n_fs):
+            proj = proj + grcv[m, d].astype(jnp.float32)
+        proj_ref[m] = proj
+        for _, l in moments[m]:
+            l.wait()
+        direction = moment_update(moments[m][0][0][...], moments[m][1][0][...], proj)[2]
+        dir_ref[m, own_ranks, :] = direction.astype(jnp.bfloat16)
+        mine = dir_ref.at[m, own_ranks]
+        out = []
+        for d in range(1, n_fs):
+            c = remote(mine, mine, d_s.at[m, d], d_r.at[m, d], fs=fs_peer(d))
+            c.start()
+            out.append(c)
+        return out
+
+    spread = [direct(0), direct(1)]
+    squares = []
+    for m in range(2):
+        for c in spread[m]:
+            c.wait_recv()
+        v = dir_ref[m]
+        gv = jnp.dot(gram[m, 0], v, preferred_element_type=jnp.float32)
+        gv = gv + jnp.dot(gram[m, 1], v, preferred_element_type=jnp.float32)
+        squares.append(jnp.sum(v.astype(jnp.float32) * gv))
+    row = lax.broadcasted_iota(jnp.int32, ssnd.shape, 0)
+    mine = jnp.where(row < SUBLANES // 2, squares[0], squares[1])
+    ssnd[...] = mine
+    tells = []
+    for d in range(1, n_tp):
+        c = remote(ssnd, srcv.at[d], s_s.at[d], s_r.at[d], tp=lax.rem(tp + d, n_tp))
+        c.start()
+        tells.append(c)
+    srcv[0] = mine
+    for c in tells:
+        c.wait_recv()
+    acc = jnp.zeros(ssnd.shape, jnp.float32)
+    for t in range(n_tp):
+        acc = acc + srcv[lax.rem(tp + n_tp - t, n_tp)]
+    scale_ref[...] = lax.rsqrt(acc / total + norm_eps)
+
+    for c in weights:
+        c.wait()
+    for m in range(2):
+        pair[m].wait_send()
+        for c in scat[m] + [c for _, c in gat[m][0]] + gat[m][1] + red[m] + spread[m]:
+            c.wait_send()
+    for c in tells:
+        c.wait_send()
+
+
+def finish_kernel(
+    scale_ref, dir_ref, bo_ref, bf_ref, wall_o, wall_f, wo_ref, wf_ref, proj_ref, mo, vo, mf, vf,
+    step_f, step_o, new_f, new_o, mf_n, vf_n, mo_n, vo_n, copy_f, copy_o, dir_t,
+):
+    k = pl.program_id(0)
+    fs = lax.axis_index("fs")
+
+    @pl.when(k == 0)
+    def _():
+        dir_t[...] = dir_ref[0].astype(jnp.float32).T.astype(jnp.bfloat16)
+        mean, var, _ = moment_update(mo[...], vo[...], proj_ref[0])
+        mo_n[...] = mean
+        vo_n[...] = var
+        mean, var, _ = moment_update(mf[...], vf[...], proj_ref[1])
+        mf_n[...] = mean
+        vf_n[...] = var
+
+    scale_o = scale_ref[0:1, 0:1]
+    scale_f = scale_ref[SUBLANES // 2 : SUBLANES // 2 + 1, 0:1]
+    upd_f = jnp.dot(bf_ref[...], dir_ref[1], preferred_element_type=jnp.float32) * scale_f
+    copy_f[...] = (wall_f[0].astype(jnp.float32) - step_rate * upd_f).astype(jnp.bfloat16)
+    upd_o = (
+        lax.dot_general(
+            dir_t[...], bo_ref[...], (((1,), (1,)), ((), ())), preferred_element_type=jnp.float32
+        )
+        * scale_o
+    )
+    copy_o[...] = (wall_o[0].astype(jnp.float32) - step_rate * upd_o).astype(jnp.bfloat16)
+
+    @pl.when(k == fs)
+    def _():
+        step_f[...] = upd_f
+        new_f[...] = wf_ref[...] - step_rate * upd_f
+        step_o[...] = upd_o
+        new_o[...] = wo_ref[...] - step_rate * upd_o
+
+
+def kernels_device(
+    n_fs, n_tp, hidden_in, forget_pre, forget_cot, lower_bound, head_out, out_cot, basis_forget, basis_output,
+    weight_forget, weight_output, mean_forget, var_forget, mean_output, var_output,
+):
+    tokens, units = head_out.shape
+    feats = hidden_in.shape[1]
+    rows = weight_forget.shape[0]
+    channels, rank = basis_forget.shape
+    part = rank // n_fs
+    n_z = n_tp // CORES
+    half = tokens // CORES
+    quarter = half // n_z
+    bf16, f32 = jnp.bfloat16, jnp.float32
+    shape = jax.ShapeDtypeStruct
+    anywhere = pl.BlockSpec(memory_space=pl.ANY)
+    vmem = pl.BlockSpec(memory_space=pltpu.VMEM)
+    dma = pltpu.SemaphoreType.DMA
+    inputs = (
+        head_out, forget_pre, forget_cot, lower_bound.reshape(1, units), basis_output, basis_forget,
+        weight_output, weight_forget, out_cot, hidden_in, mean_output, var_output, mean_forget, var_forget,
+    )
+    directions, proj, scale, wall_o, wall_f = pl.pallas_call(
+        functools.partial(comm_kernel, n_fs, n_tp, float(channels * feats * n_tp)),
+        out_shape=(
+            shape((2, rank, feats), bf16),
+            shape((2, part, feats), f32),
+            shape((SUBLANES, LANES), f32),
+            shape((n_fs,) + weight_output.shape, bf16),
+            shape((n_fs,) + weight_forget.shape, bf16),
+        ),
+        in_specs=[anywhere] * 3 + [vmem] + [anywhere] * 10,
+        out_specs=(vmem, vmem, vmem, anywhere, anywhere),
+        scratch_shapes=[
+            pltpu.VMEM(a.shape, a.dtype)
+            for a in (
+                head_out, forget_pre, forget_cot, basis_output, basis_forget, weight_output, weight_forget,
+                out_cot, hidden_in, mean_output, var_output, mean_forget, var_forget,
+            )
+        ]
+        + [
+            pltpu.VMEM((2, half, rank), f32),
+            pltpu.VMEM((2, half, rank), bf16),
+            pltpu.VMEM((2, half, rank), bf16),
+            pltpu.VMEM((2, half, rank), bf16),
+            pltpu.VMEM((2, n_z, quarter, rank), bf16),
+            pltpu.VMEM((2, tokens, rank), bf16),
+            pltpu.VMEM((2, rank, feats), bf16),
+            pltpu.VMEM((2, n_fs, part, feats), bf16),
+            pltpu.VMEM((2, rank, feats), f32),
+            pltpu.VMEM((2,) + weight_forget.shape, bf16),
+            pltpu.VMEM((SUBLANES, LANES), f32),
+            pltpu.VMEM((n_tp, SUBLANES, LANES), f32),
+            pltpu.VMEM((2, 2, rank, rank), bf16),
+            dma((13,)),
+            dma((2,)), dma((2,)),
+            dma((2, n_z)), dma((2, n_z)), dma((2, n_z)), dma((2, n_z)), dma((2, n_z)), dma((2, n_z)),
+            dma((2, n_fs)), dma((2, n_fs)), dma((2, n_fs)), dma((2, n_fs)), dma((2, n_fs)), dma((2, n_fs)),
+            dma((2,)),
+            dma((n_tp,)), dma((n_tp,)),
+        ],
+        compiler_params=pltpu.CompilerParams(
+            collective_id=0, has_side_effects=True, vmem_limit_bytes=60 * 2**20
+        ),
+    )(*inputs)
+
+    def whole(a):
+        return pl.BlockSpec(a.shape, lambda k, n=len(a.shape): (0,) * n)
+
+    def outs(a):
+        return whole(shape(a.shape, f32))
+
+    outputs = pl.pallas_call(
+        finish_kernel,
+        grid=(n_fs,),
+        out_shape=tuple(
+            shape(a.shape, f32)
+            for a in (
+                weight_forget, weight_output, weight_forget, weight_output, mean_forget, var_forget,
+                mean_output, var_output,
+            )
+        )
+        + (shape((channels, feats), bf16), shape((feats, channels), bf16)),
+        in_specs=[
+            whole(scale),
+            whole(directions),
+            pl.BlockSpec((rows, rank), lambda k: (k, 0)),
+            pl.BlockSpec((rows, rank), lambda k: (k, 0)),
+            pl.BlockSpec((1,) + weight_output.shape, lambda k: (k, 0, 0)),
+            pl.BlockSpec((1,) + weight_forget.shape, lambda k: (k, 0, 0)),
+            whole(weight_output),
+            whole(weight_forget),
+            whole(proj),
+            whole(mean_output),
+            whole(var_output),
+            whole(mean_forget),
+            whole(var_forget),
+        ],
+        out_specs=tuple(
+            outs(a)
+            for a in (
+                weight_forget, weight_output, weight_forget, weight_output, mean_forget, var_forget,
+                mean_output, var_output,
+            )
+        )
+        + (
+            pl.BlockSpec((rows, feats), lambda k: (k, 0)),
+            pl.BlockSpec((feats, rows), lambda k: (0, k)),
+        ),
+        scratch_shapes=[pltpu.VMEM((feats, rank), bf16)],
+        compiler_params=pltpu.CompilerParams(
+            dimension_semantics=("arbitrary",), vmem_limit_bytes=48 * 2**20
+        ),
+    )(
+        scale, directions, basis_output, basis_forget, wall_o, wall_f, weight_output, weight_forget, proj,
+        mean_output, var_output, mean_forget, var_forget,
+    )
+    return outputs
 
 
 def split_product(coords, tokens_data):
@@ -80,7 +501,7 @@
     )
     upd_forget = jnp.dot(rows_forget, dir_forget, precision=highest)
     upd_output = jnp.dot(rows_output, dir_output, precision=highest)
-    total = float(HW * D)
+    total = float(basis_forget.shape[0] * feat_cols * lax.axis_size("tp"))
     sum_forget, sum_output = lax.psum(
         (jnp.sum(upd_forget * upd_forget), jnp.sum(upd_output * upd_output)), ("fs", "tp")
     )
@@ -106,9 +527,31 @@
     )
 
 
+def fits(n_fs, n_tp, forget_pre, hidden_in, basis):
+    tokens, units = forget_pre.shape
+    quarter = tokens // n_tp
+    part = basis.shape[1] // n_fs
+    return (
+        n_tp % CORES == 0
+        and n_tp > CORES
+        and n_fs > 1
+        and tokens % n_tp == 0
+        and units % LANES == 0
+        and hidden_in.shape[1] % LANES == 0
+        and quarter % (2 * SUBLANES) == 0
+        and part % (2 * SUBLANES) == 0
+    )
+
+
+def device_step(n_fs, n_tp, *args):
+    if fits(n_fs, n_tp, args[1], args[0], args[6]):
+        return kernels_device(n_fs, n_tp, *args)
+    return per_device(*args)
+
+
 def solution(mesh):
     return jax.shard_map(
-        per_device,
+        functools.partial(device_step, mesh.shape["fs"], mesh.shape["tp"]),
         mesh=mesh,
         in_specs=(
             P("fs", "tp"),

time: 283 us -> 86.2 us (0.30)
  waiting for transfers between devices: 175 us -> 0 us
  Pallas kernels: 0 us -> 81.2 us
  blocking collectives: 59.3 us -> 0 us
  matrix products: 15.1 us -> 0 us
  between operations: 15.3 us -> 0.78 us
  other arithmetic: 9.91 us -> 0 us
  local copies, waits for them, and re-layouts: 7.41 us -> 3.91 us
    pallas_call x0 -> x2, Pallas kernels: none -> 81.2 us  [the longest x1 73.4 us: kernels_device(): pl.pallas_call(functools.partial(comm_kernel, n_fs, n_tp, float(channels...]
    psum x1 -> x0, waiting for transfers between devices: 79.7 us -> none  [per_device(): lax.psum((coords_forget, coords_output), 'tp')]
    all_gather x2 -> x0, waiting for transfers between devices: 67.5 us -> none  [the longest x1 37.3 us: per_device(): lax.all_gather(new_output.astype(jnp.bfloat16), 'fs', axis=1, tiled=True)]
    psum x1 -> x0, blocking collectives: 39.5 us -> none  [per_device(): lax.psum((jnp.sum(upd_forget * upd_forget), jnp.sum(upd_output * upd_outp...]
    reduce_scatter x1 -> x0, waiting for transfers between devices: 28 us -> none  [per_device(): lax.psum_scatter(jnp.concatenate([part_forget, part_output], axis=1), 'fs...]
    all_gather x2 -> x0, blocking collectives: 19.8 us -> none  [the longest x1 10.1 us: per_device(): lax.all_gather(dir_output, 'fs', axis=0, tiled=True)]
    dot_general x8 -> x0, matrix products: 15.1 us -> none  [the longest x1 3.16 us: per_device(): upd_output = jnp.dot(rows_output, dir_output, precision=highest)]
    convert_element_type x2 -> x0, other arithmetic: 6.16 us -> none  [the longest x1 3.08 us: per_device(): new_forget.astype(jnp.bfloat16)]
  transfers between devices with their start and end apart: 4 -> 0, of which waited for: 4 -> 0; matrix products, arithmetic and copies ran while one was open for 2% -> 0% of each run, Pallas kernels for 0% -> 0%
where the time goes in v1:
time: 86.2 us; the launch traced here: 85.9 us
  Pallas kernels  81.2 us (94%)
  local copies, waits for them, and re-layouts  3.91 us (5%)
    pallas_call x1, Pallas kernels, kernels_device(): pl.pallas_call(functools.partial(comm_kernel, n_fs, n_tp, float(channels...  73.4 us
    pallas_call x1, Pallas kernels, kernels_device(): pl.pallas_call(finish_kernel, grid=(n_fs,), out_shape=tuple((shape(a.shap...  7.8 us
    unnamed x22, local copies, waits for them, and re-layouts  3.91 us

profile of v1, /device:TPU:0, one launch (start us, length us, event | category | flops | bytes accessed | tf_op | source)
XLA Modules:
  0.0 85.9 jit_solution(2930977660804857833)
XLA Ops:
  0.6 0.0 copy-start
  0.7 0.0 copy-start.1
  0.7 0.0 copy-start.2
  0.7 0.0 copy-start.4
  0.7 0.0 copy-start.5
  0.7 0.0 copy-start.6
  0.7 0.0 copy-start.7
  0.7 73.4 %shard_map.213 = (bf16[2,256,512]{2,1,0:T(8,128)(2,1)}, f32[2,64,512]{2,1,0:T(8,128)}, f32[8,128]{1,0:T(8,128)}, bf16[4,512,512]{2,1,0:T(8,128)(2,1)}, bf16[4,512,512]{2,1,0:T(8,128)(2,1)}) custom-call(bf16[1536,256]{1,0:T(8,128)(2,1)} %ho_h.1, bf16[1536,256]{1,0:T(8,128)(2,1)} %fp_h.1, bf16[1536,256]{1,0:T(8,128)(2,1)} %fc_h.1, f32[1,256]{1,0:T(1,128)} %bitcast.1, ...), custom_call_target="tpu_custom_call" | custom-call | tf_op jit(solution)/shard_map/pallas_call | solution.py:346
  74.1 0.0 copy-done
  74.1 0.0 copy-done.1
  74.1 0.0 copy-done.2
  74.1 0.0 copy-done.4
  74.2 0.0 copy-done.5
  74.2 0.0 copy-done.6
  74.2 0.0 copy-done.7
  74.2 0.0 copy-start.3
  74.2 1.2 %copy-done.3 = f32[512,512]{1,0:T(8,128)S(1)} copy-done((f32[512,512]{1,0:T(8,128)S(1)}, f32[512,512]{1,0:T(8,128)}, u32[]{:S(2)}) %copy-start.3) | copy-done | bytes 1048600
  75.4 0.0 copy-start.8
  75.4 1.0 %copy-done.8 = bf16[2,256,512]{2,1,0:T(8,128)(2,1)S(1)} copy-done((bf16[2,256,512]{2,1,0:T(8,128)(2,1)S(1)}, bf16[2,256,512]{2,1,0:T(8,128)(2,1)}, u32[]{:S(2)}) %copy-start.8) | copy-done | bytes 524312
  76.5 0.0 copy-start.9
  76.5 0.9 %copy-done.9 = f32[2,64,512]{2,1,0:T(8,128)S(1)} copy-done((f32[2,64,512]{2,1,0:T(8,128)S(1)}, f32[2,64,512]{2,1,0:T(8,128)}, u32[]{:S(2)}) %copy-start.9) | copy-done | bytes 262168
  77.4 0.0 copy-start.10
  77.4 0.7 copy-done.10
  78.1 7.8 %shard_map.214 = (f32[512,512]{1,0:T(8,128)}, f32[512,512]{1,0:T(8,128)}, f32[512,512]{1,0:T(8,128)}, f32[512,512]{1,0:T(8,128)}, f32[64,512]{1,0:T(8,128)}, /*i...) custom-call(f32[8,128]{1,0:T(8,128)S(1)} %copy-done.10, ...), custom_call_target="tpu_custom_call" | custom-call | tf_op jit(solution)/shard_map/pallas_call | solution.py:396
Async XLA Ops:
  0.6 73.5 %copy-start = (bf16[2048,256]{1,0:T(8,128)(2,1)S(1)}, bf16[2048,256]{1,0:T(8,128)(2,1)}, u32[]{:S(2)}) copy-start(bf16[2048,256]{1,0:T(8,128)(2,1)} %bo_ref.1) | copy-start | bytes 3145732
  0.7 73.5 %copy-start.1 = (bf16[2048,256]{1,0:T(8,128)(2,1)S(1)}, bf16[2048,256]{1,0:T(8,128)(2,1)}, u32[]{:S(2)}) copy-start(bf16[2048,256]{1,0:T(8,128)(2,1)} %bf_ref.1) | copy-start | bytes 3145732
  0.7 73.5 %copy-start.2 = (f32[512,512]{1,0:T(8,128)S(1)}, f32[512,512]{1,0:T(8,128)}, u32[]{:S(2)}) copy-start(f32[512,512]{1,0:T(8,128)} %wo_ref.1) | copy-start | bytes 3145732
  0.7 73.5 %copy-start.4 = (f32[64,512]{1,0:T(8,128)S(1)}, f32[64,512]{1,0:T(8,128)}, u32[]{:S(2)}) copy-start(f32[64,512]{1,0:T(8,128)} %mo.1) | copy-start | bytes 393220
  0.7 73.5 %copy-start.5 = (f32[64,512]{1,0:T(8,128)S(1)}, f32[64,512]{1,0:T(8,128)}, u32[]{:S(2)}) copy-start(f32[64,512]{1,0:T(8,128)} %vo.1) | copy-start | bytes 393220
  0.7 73.5 %copy-start.6 = (f32[64,512]{1,0:T(8,128)S(1)}, f32[64,512]{1,0:T(8,128)}, u32[]{:S(2)}) copy-start(f32[64,512]{1,0:T(8,128)} %mf.1) | copy-start | bytes 393220
  0.7 73.5 %copy-start.7 = (f32[64,512]{1,0:T(8,128)S(1)}, f32[64,512]{1,0:T(8,128)}, u32[]{:S(2)}) copy-start(f32[64,512]{1,0:T(8,128)} %vf.1) | copy-start | bytes 393220
  74.2 1.2 %copy-start.3 = (f32[512,512]{1,0:T(8,128)S(1)}, f32[512,512]{1,0:T(8,128)}, u32[]{:S(2)}) copy-start(f32[512,512]{1,0:T(8,128)} %wf_ref.1) | copy-start | bytes 3145732
  75.4 1.0 %copy-start.8 = (bf16[2,256,512]{2,1,0:T(8,128)(2,1)S(1)}, bf16[2,256,512]{2,1,0:T(8,128)(2,1)}, u32[]{:S(2)}) copy-start(bf16[2,256,512]{2,1,0:T(8,128)(2,1)} %get-tuple-element.16.dir_ref) | copy-start | bytes 1572868
  76.5 0.9 %copy-start.9 = (f32[2,64,512]{2,1,0:T(8,128)S(1)}, f32[2,64,512]{2,1,0:T(8,128)}, u32[]{:S(2)}) copy-start(f32[2,64,512]{2,1,0:T(8,128)} %get-tuple-element.19.proj_ref) | copy-start | bytes 786436
  77.4 0.7 copy-start.10

commit v2 on v1

--- a/solution.py
+++ b/solution.py
@@ -62,11 +62,11 @@
     loads = [
         pltpu.make_async_copy(s, d, ld.at[i])
         for i, (s, d) in enumerate((
-            (ho_h, ho), (bo_h, bo), (wo_h, wo), (wf_h, wf), (fp_h, fp), (fc_h, fc), (bf_h, bf),
+            (ho_h, ho), (bo_h, bo), (fp_h, fp), (fc_h, fc), (bf_h, bf), (wo_h, wo), (wf_h, wf),
             (oc_h, oc), (hi_h, hi), (mo_h, mo), (vo_h, vo), (mf_h, mf), (vf_h, vf),
         ))
     ]
-    (l_ho, l_bo, l_wo, l_wf, l_fp, l_fc, l_bf, l_oc, l_hi, l_mo, l_vo, l_mf, l_vf) = loads
+    (l_ho, l_bo, l_fp, l_fc, l_bf, l_wo, l_wf, l_oc, l_hi, l_mo, l_vo, l_mf, l_vf) = loads
     for l in loads:
         l.start()
 
@@ -76,11 +76,6 @@
     for d in range(1, n_fs):
         pl.semaphore_signal(barrier, inc=1, device_id={"fs": fs_peer(d)}, device_id_type=MESH)
 
-    l_wo.wait()
-    wsnd[0] = wo[...].astype(jnp.bfloat16)
-    l_wf.wait()
-    wsnd[1] = wf[...].astype(jnp.bfloat16)
-
     def rows_at(which, i):
         return pl.ds(pl.multiple_of(which * half + i * quarter, quarter), quarter)
 
@@ -92,10 +87,6 @@
 
     def coord_o(which, i):
         return jnp.dot(ho[rows_at(which, i), :], local_rows(bo), preferred_element_type=jnp.float32)
-
-    l_fp.wait()
-    l_fc.wait()
-    l_bf.wait()
 
     def coord_f(which, i):
         rows = rows_at(which, i)
@@ -125,18 +116,51 @@
 
     away(0)
     pl.semaphore_wait(barrier, n_tp - 1 + n_fs - 1)
-    weights = []
-    for m, wall in ((0, wall_o), (1, wall_f)):
-        for d in range(1, n_fs):
-            c = remote(wsnd.at[m], wall.at[fs], w_s.at[m, d], w_r.at[m, d], fs=fs_peer(d))
-            weights.append(c)
-            c.start()
-        c = pltpu.make_async_copy(wsnd.at[m], wall.at[fs], wl.at[m])
-        c.start()
-        weights.append(c)
     pair[0].start()
+
+    x, y = lax.rem(fs, 2), fs // 2
+    beside, above = y * 2 + 1 - x, (1 - y) * 2 + x
+    walls = (wall_o, wall_f)
+
+    def send_weights(m):
+        wall = walls[m]
+        load, source = ((l_wo, wo), (l_wf, wf))[m]
+        load.wait()
+        wsnd[m] = source[...].astype(jnp.bfloat16)
+        sent = []
+        if n_fs == 4:
+            peers = (beside, above)
+        else:
+            peers = [fs_peer(d) for d in range(1, n_fs)]
+        for i, peer in enumerate(peers):
+            c = remote(wsnd.at[m], wall.at[fs], w_s.at[m, i], w_r.at[m, i], fs=peer)
+            c.start()
+            sent.append(c)
+        kept = pltpu.make_async_copy(wsnd.at[m], wall.at[fs], wl.at[m])
+        kept.start()
+        return sent, kept
+
+    def relay_weights(m):
+        if n_fs != 4:
+            return []
+        sent = weights[m][0]
+        rows = walls[m].shape[1] // 2
+        passed = []
+        for i, (origin, target) in enumerate(((beside, above), (above, beside))):
+            sent[i].wait_recv()
+            piece = walls[m].at[origin, pl.ds(i * rows, rows)]
+            c = remote(piece, piece, w_s.at[m, 2 + i], w_r.at[m, 2 + i], fs=target)
+            c.start()
+            passed.append(c)
+        return passed
+
+    weights = [send_weights(0)]
+    l_fp.wait()
+    l_fc.wait()
+    l_bf.wait()
     away(1)
     pair[1].start()
+    weights.append(send_weights(1))
     home(0)
 
     def chunk(ref, m, j):
@@ -198,7 +222,10 @@
         f.start()
         return sends, [f]
 
-    gat = [gather(0), gather(1)]
+    gat = [gather(0)]
+    passed = [relay_weights(0)]
+    gat.append(gather(1))
+    passed.append(relay_weights(1))
 
     data = ((oc, l_oc), (hi, l_hi))
 
@@ -275,9 +302,14 @@
         acc = acc + srcv[lax.rem(tp + n_tp - t, n_tp)]
     scale_ref[...] = lax.rsqrt(acc / total + norm_eps)
 
-    for c in weights:
-        c.wait()
     for m in range(2):
+        for c in weights[m][0]:
+            if n_fs != 4:
+                c.wait_recv()
+            c.wait_send()
+        weights[m][1].wait()
+        for c in passed[m]:
+            c.wait()
         pair[m].wait_send()
         for c in scat[m] + [c for _, c in gat[m][0]] + gat[m][1] + red[m] + spread[m]:
             c.wait_send()
@@ -286,14 +318,23 @@
 
 
 def finish_kernel(
-    scale_ref, dir_ref, bo_ref, bf_ref, wall_o, wall_f, wo_ref, wf_ref, proj_ref, mo, vo, mf, vf,
-    step_f, step_o, new_f, new_o, mf_n, vf_n, mo_n, vo_n, copy_f, copy_o, dir_t,
+    fs_ref, scale_ref, dir_ref, bo_ref, bf_ref, wall_o, wall_f, wo_h, wf_h, proj_ref, mo, vo, mf, vf,
+    step_f_h, step_o_h, new_f_h, new_o_h, mf_n, vf_n, mo_n, vo_n, copy_f, copy_o,
+    dir_t, wo, wf, step_f, step_o, new_f, new_o, in_sem, out_sem,
 ):
     k = pl.program_id(0)
-    fs = lax.axis_index("fs")
+    reads = [pltpu.make_async_copy(s, d, in_sem.at[i]) for i, (s, d) in enumerate(((wo_h, wo), (wf_h, wf)))]
+    writes = [
+        pltpu.make_async_copy(s, d, out_sem.at[i])
+        for i, (s, d) in enumerate(
+            ((step_f, step_f_h), (step_o, step_o_h), (new_f, new_f_h), (new_o, new_o_h))
+        )
+    ]
 
     @pl.when(k == 0)
     def _():
+        for c in reads:
+            c.start()
         dir_t[...] = dir_ref[0].astype(jnp.float32).T.astype(jnp.bfloat16)
         mean, var, _ = moment_update(mo[...], vo[...], proj_ref[0])
         mo_n[...] = mean
@@ -314,12 +355,21 @@
     )
     copy_o[...] = (wall_o[0].astype(jnp.float32) - step_rate * upd_o).astype(jnp.bfloat16)
 
-    @pl.when(k == fs)
+    @pl.when(k == 1)
     def _():
+        for c in reads:
+            c.wait()
         step_f[...] = upd_f
-        new_f[...] = wf_ref[...] - step_rate * upd_f
         step_o[...] = upd_o
-        new_o[...] = wo_ref[...] - step_rate * upd_o
+        new_f[...] = wf[...] - step_rate * upd_f
+        new_o[...] = wo[...] - step_rate * upd_o
+        for c in writes:
+            c.start()
+
+    @pl.when(k == pl.num_programs(0) - 1)
+    def _():
+        for c in writes:
+            c.wait()
 
 
 def kernels_device(
@@ -388,53 +438,50 @@
     )(*inputs)
 
     def whole(a):
-        return pl.BlockSpec(a.shape, lambda k, n=len(a.shape): (0,) * n)
-
-    def outs(a):
-        return whole(shape(a.shape, f32))
-
+        return pl.BlockSpec(a.shape, lambda k, r, n=len(a.shape): (0,) * n)
+
+    def turn(k, r):
+        return lax.rem(k + r[0] + n_fs - 1, n_fs)
+
+    f32_weights = (weight_forget, weight_output, weight_forget, weight_output)
+    f32_moments = (mean_forget, var_forget, mean_output, var_output)
     outputs = pl.pallas_call(
         finish_kernel,
-        grid=(n_fs,),
-        out_shape=tuple(
-            shape(a.shape, f32)
-            for a in (
-                weight_forget, weight_output, weight_forget, weight_output, mean_forget, var_forget,
-                mean_output, var_output,
-            )
-        )
+        grid_spec=pltpu.PrefetchScalarGridSpec(
+            num_scalar_prefetch=1,
+            grid=(n_fs,),
+            in_specs=[
+                whole(scale),
+                whole(directions),
+                pl.BlockSpec((rows, rank), lambda k, r: (turn(k, r), 0)),
+                pl.BlockSpec((rows, rank), lambda k, r: (turn(k, r), 0)),
+                pl.BlockSpec((1,) + weight_output.shape, lambda k, r: (turn(k, r), 0, 0)),
+                pl.BlockSpec((1,) + weight_forget.shape, lambda k, r: (turn(k, r), 0, 0)),
+                anywhere,
+                anywhere,
+                whole(proj),
+                whole(mean_output),
+                whole(var_output),
+                whole(mean_forget),
+                whole(var_forget),
+            ],
+            out_specs=[anywhere] * 4
+            + [whole(a) for a in f32_moments]
+            + [
+                pl.BlockSpec((rows, feats), lambda k, r: (turn(k, r), 0)),
+                pl.BlockSpec((feats, rows), lambda k, r: (0, turn(k, r))),
+            ],
+            scratch_shapes=[pltpu.VMEM((feats, rank), bf16)]
+            + [pltpu.VMEM(a.shape, f32) for a in (weight_output, weight_forget) + f32_weights]
+            + [dma((2,)), dma((4,))],
+        ),
+        out_shape=tuple(shape(a.shape, f32) for a in f32_weights + f32_moments)
         + (shape((channels, feats), bf16), shape((feats, channels), bf16)),
-        in_specs=[
-            whole(scale),
-            whole(directions),
-            pl.BlockSpec((rows, rank), lambda k: (k, 0)),
-            pl.BlockSpec((rows, rank), lambda k: (k, 0)),
-            pl.BlockSpec((1,) + weight_output.shape, lambda k: (k, 0, 0)),
-            pl.BlockSpec((1,) + weight_forget.shape, lambda k: (k, 0, 0)),
-            whole(weight_output),
-            whole(weight_forget),
-            whole(proj),
-            whole(mean_output),
-            whole(var_output),
-            whole(mean_forget),
-            whole(var_forget),
-        ],
-        out_specs=tuple(
-            outs(a)
-            for a in (
-                weight_forget, weight_output, weight_forget, weight_output, mean_forget, var_forget,
-                mean_output, var_output,
-            )
-        )
-        + (
-            pl.BlockSpec((rows, feats), lambda k: (k, 0)),
-            pl.BlockSpec((feats, rows), lambda k: (0, k)),
-        ),
-        scratch_shapes=[pltpu.VMEM((feats, rank), bf16)],
         compiler_params=pltpu.CompilerParams(
-            dimension_semantics=("arbitrary",), vmem_limit_bytes=48 * 2**20
+            dimension_semantics=("arbitrary",), vmem_limit_bytes=63 * 2**20
         ),
     )(
+        lax.axis_index("fs").reshape(1).astype(jnp.int32),
         scale, directions, basis_output, basis_forget, wall_o, wall_f, weight_output, weight_forget, proj,
         mean_output, var_output, mean_forget, var_forget,
     )

time: 86.2 us -> 70.5 us (0.82)
  Pallas kernels: 81.2 us -> 69.6 us
  local copies, waits for them, and re-layouts: 3.91 us -> 0 us
    pallas_call x1, Pallas kernels: 73.4 us -> 61.3 us  [kernels_device(): pl.pallas_call(functools.partial(comm_kernel, n_fs, n_tp, float(channels...]
    unnamed x22 -> x0, local copies, waits for them, and re-layouts: 3.91 us -> none
where the time goes in v2:
time: 70.5 us; the launch traced here: 70.3 us
  Pallas kernels  69.6 us (99%)
    pallas_call x1, Pallas kernels, kernels_device(): pl.pallas_call(functools.partial(comm_kernel, n_fs, n_tp, float(channels...  61.3 us
    pallas_call x1, Pallas kernels, kernels_device(): pl.pallas_call(finish_kernel, grid_spec=pltpu.PrefetchScalarGridSpec(num_...  8.33 us

profile of v2, /device:TPU:0, one launch (start us, length us, event | category | flops | bytes accessed | tf_op | source)
XLA Modules:
  0.0 70.3 jit_solution(8926650516970574917)
XLA Ops:
  0.6 61.3 %shard_map.213 = (bf16[2,256,512]{2,1,0:T(8,128)(2,1)}, f32[2,64,512]{2,1,0:T(8,128)}, f32[8,128]{1,0:T(8,128)}, bf16[4,512,512]{2,1,0:T(8,128)(2,1)}, bf16[4,512,512]{2,1,0:T(8,128)(2,1)}) custom-call(bf16[1536,256]{1,0:T(8,128)(2,1)} %ho_h.1, bf16[1536,256]{1,0:T(8,128)(2,1)} %fp_h.1, bf16[1536,256]{1,0:T(8,128)(2,1)} %fc_h.1, f32[1,256]{1,0:T(1,128)} %bitcast.2, ...), custom_call_target="tpu_custom_call" | custom-call | tf_op jit(solution)/shard_map/pallas_call | solution.py:396
  62.0 8.3 %shard_map.214 = (f32[512,512]{1,0:T(8,128)}, f32[512,512]{1,0:T(8,128)}, f32[512,512]{1,0:T(8,128)}, f32[512,512]{1,0:T(8,128)}, f32[64,512]{1,0:T(8,128)}, /*i...) custom-call(s32[1]{0:T(128)} %bitcast.fs_ref, ...), custom_call_target="tpu_custom_call" | custom-call | tf_op jit(solution)/shard_map/pallas_call | solution.py:448
